TPU v7x, 32 devices: a whole 2x2x4 slice. The times are simulated.
32 devices in a mesh: dp: 4 (over y, x), kv: 4 (over z), tp: 2 (over core).
Axes of the slice: x: 2, y: 2, z: 4, core: 2. Of those that a mesh axis runs over, the one named last changes fastest.
Arguments:
- tokens: bfloat16 [16, 4096], P('dp', ('kv', 'tp')), parts along dimension 0, may hold values from -6 to 6
- mix_gain: float32 [4096], replicated, may hold values from 0.1 to 1.9
- w_query: bfloat16 [4096, 2048], P('kv', 'tp'), may hold values from -0.09375 to 0.09375
- w_key: bfloat16 [4096, 2048], P('kv', 'tp'), may hold values from -0.09375 to 0.09375
- w_value: bfloat16 [4096, 4096], P('kv', 'tp'), may hold values from -0.09375 to 0.09375
- w_igate: bfloat16 [4096, 16], replicated, may hold values from -0.09375 to 0.09375
- w_fgate: bfloat16 [4096, 16], replicated, may hold values from -0.09375 to 0.09375
- igate_bias: float32 [16], replicated, may hold values from -3 to 1
- fgate_bias: float32 [16], replicated, may hold values from -2 to 5
- memory: float32 [16, 16, 256, 128], P(('dp', 'kv'), 'tp'), parts along dimension 0, may hold values from -6 to 6
- normalizer: float32 [16, 16, 128], P(('dp', 'kv'), 'tp'), parts along dimension 0, may hold values from -6 to 6
- stabilizer: float32 [16, 16], P(('dp', 'kv'), 'tp'), parts along dimension 0, may hold values from -3 to 3
- w_output: bfloat16 [4096, 4096], P('tp', 'kv'), may hold values from -0.09375 to 0.09375
- mlp_gain: float32 [4096], replicated, may hold values from 0.1 to 1.9
- w_up: bfloat16 [4096, 16384], P(None, ('kv', 'tp')), may hold values from -0.09375 to 0.09375
- w_down: bfloat16 [16384, 4096], P(('kv', 'tp')), may hold values from -0.0625 to 0.0625
Outputs:
- new_tokens: bfloat16 [16, 4096], P('dp', ('kv', 'tp')), parts along dimension 0
- new_memory: float32 [16, 16, 256, 128], P(('dp', 'kv'), 'tp'), parts along dimension 0
- new_normalizer: float32 [16, 16, 128], P(('dp', 'kv'), 'tp'), parts along dimension 0
- new_stabilizer: float32 [16, 16], P(('dp', 'kv'), 'tp'), parts along dimension 0
There are 4 independent parts, one for each index of `dp`. A program takes and returns all parts, laid end to end along the dimension named above; an argument that names none is the same for every part. Nothing has to cross between parts.
All inputs are finite; a program needn't handle non-finite values.
Results may differ from a plain program's by a relative error of at most 0.019.
Values may be sent and summed in bfloat16 or wider, within the bound.
A program may use at most 128 MiB of HBM per device.

v0:
```python
import jax
import jax.numpy as jnp
from jax import lax
from jax.sharding import PartitionSpec as P

DV = 256
DQK = 128


norm_eps = 1e-06


def rms_normed(rows, gain):
    wide_rows = rows.astype(jnp.float32)
    scale = lax.rsqrt(jnp.mean(wide_rows * wide_rows, axis=-1, keepdims=True) + norm_eps)
    return (wide_rows * scale * gain).astype(jnp.bfloat16)


def on_device(
    tokens,
    mix_gain,
    w_query,
    w_key,
    w_value,
    w_igate,
    w_fgate,
    igate_bias,
    fgate_bias,
    memory,
    normalizer,
    stabilizer,
    w_output,
    mlp_gain,
    w_up,
    w_down,
):
    kv_count = lax.axis_size("kv")
    tp_count = lax.axis_size("tp")
    kv_index = lax.axis_index("kv")
    tp_index = lax.axis_index("tp")
    own_rows = memory.shape[0]
    head_count = memory.shape[1]
    whole_rows = lax.all_gather(tokens, ("kv", "tp"), axis=1, tiled=True)
    batch_rows = whole_rows.shape[0]
    wide_rows = whole_rows.astype(jnp.float32)
    normed = rms_normed(whole_rows, mix_gain)
    row_span = w_query.shape[0]
    own_cols = lax.dynamic_slice_in_dim(normed, kv_index * row_span, row_span, 1)
    joined = lax.psum_scatter(
        jnp.concatenate(
            [
                jnp.dot(own_cols, w_query, preferred_element_type=jnp.float32),
                jnp.dot(own_cols, w_key, preferred_element_type=jnp.float32),
                jnp.dot(own_cols, w_value, preferred_element_type=jnp.float32),
            ],
            axis=1,
        ),
        "kv",
        scatter_dimension=0,
        tiled=True,
    )
    query_cols = w_query.shape[1]
    queries = joined[:, :query_cols].reshape(own_rows, head_count, DQK) * DQK ** (-0.5)
    key_rows = joined[:, query_cols : 2 * query_cols].reshape(own_rows, head_count, DQK)
    values = joined[:, 2 * query_cols :].reshape(own_rows, head_count, DV)
    own_normed = lax.dynamic_slice_in_dim(normed, kv_index * own_rows, own_rows, 0)
    igate_cols = lax.dynamic_slice_in_dim(w_igate, tp_index * head_count, head_count, 1)
    fgate_cols = lax.dynamic_slice_in_dim(w_fgate, tp_index * head_count, head_count, 1)
    ibias_own = lax.dynamic_slice_in_dim(igate_bias, tp_index * head_count, head_count, 0)
    fbias_own = lax.dynamic_slice_in_dim(fgate_bias, tp_index * head_count, head_count, 0)
    input_gate = jnp.dot(own_normed, igate_cols, preferred_element_type=jnp.float32) + ibias_own
    log_forget = jax.nn.log_sigmoid(
        jnp.dot(own_normed, fgate_cols, preferred_element_type=jnp.float32) + fbias_own
    )
    carried = log_forget + stabilizer
    new_stabilizer = jnp.maximum(carried, input_gate)
    keep_weight = jnp.exp(carried - new_stabilizer)
    fresh_weight = jnp.exp(input_gate - new_stabilizer)
    recall = jnp.einsum("bhvd,bhd->bhv", memory, queries, precision=lax.Precision.HIGHEST)
    match_score = jnp.sum(queries * key_rows, axis=-1)
    numerator = keep_weight[..., None] * recall + (fresh_weight * match_score)[..., None] * values
    denominator = keep_weight * jnp.sum(normalizer * queries, axis=-1) + fresh_weight * match_score
    floor_value = jnp.maximum(jnp.abs(denominator), jnp.exp(-new_stabilizer))
    cell_out = (
        (numerator / floor_value[..., None]).astype(jnp.bfloat16).reshape(own_rows, head_count * DV)
    )
    new_memory = (
        keep_weight[..., None, None] * memory
        + fresh_weight[..., None, None] * values[..., :, None] * key_rows[..., None, :]
    )
    new_normalizer = keep_weight[..., None] * normalizer + fresh_weight[..., None] * key_rows
    partial_value = jnp.dot(
        lax.all_gather(cell_out, "kv", axis=0, tiled=True),
        w_output,
        preferred_element_type=jnp.float32,
    )
    block_cols = partial_value.shape[1]
    pieces = lax.all_gather(
        partial_value.astype(jnp.bfloat16)[:, None, :], ("kv", "tp"), axis=1, tiled=True
    )
    summed = jnp.sum(
        pieces.astype(jnp.float32).reshape(batch_rows, kv_count, tp_count, block_cols), axis=2
    )
    middle = (wide_rows + summed.reshape(batch_rows, kv_count * block_cols)).astype(jnp.bfloat16)
    mixer_in = rms_normed(middle, mlp_gain)
    up_rows = jnp.dot(mixer_in, w_up, preferred_element_type=jnp.float32)
    activation = jnp.square(jax.nn.relu(up_rows)).astype(jnp.bfloat16)
    thin_cols = tokens.shape[1]
    down_cols = lax.psum_scatter(
        lax.dot_general(
            w_down, activation, (((0,), (1,)), ((), ())), preferred_element_type=jnp.float32
        ),
        ("kv", "tp"),
        scatter_dimension=0,
        tiled=True,
    )
    middle_own = lax.dynamic_slice_in_dim(
        middle, (kv_index * tp_count + tp_index) * thin_cols, thin_cols, 1
    )
    new_tokens = (middle_own.astype(jnp.float32) + down_cols.T).astype(jnp.bfloat16)
    return (new_tokens, new_memory, new_normalizer, new_stabilizer)


def solution(mesh):
    in_specs = (
        P("dp", ("kv", "tp")),
        P(),
        P("kv", "tp"),
        P("kv", "tp"),
        P("kv", "tp"),
        P(),
        P(),
        P(),
        P(),
        P(("dp", "kv"), "tp", None, None),
        P(("dp", "kv"), "tp", None),
        P(("dp", "kv"), "tp"),
        P("tp", "kv"),
        P(),
        P(None, ("kv", "tp")),
        P(("kv", "tp"), None),
    )
    out_specs = (
        P("dp", ("kv", "tp")),
        P(("dp", "kv"), "tp", None, None),
        P(("dp", "kv"), "tp", None),
        P(("dp", "kv"), "tp"),
    )
    return jax.shard_map(
        on_device, mesh=mesh, in_specs=in_specs, out_specs=out_specs, check_vma=False
    )
```

profile of v0, /device:TPU:0, one launch (start us, length us, event | category | flops | bytes accessed | tf_op | source)
XLA Modules:
  0.0 158.9 jit_solution(7164045626821593483)
XLA Ops:
  7.2 16.1 %all_gather.9 = bf16[4,4096]{1,0:T(4,128)(2,1)S(1)} all-gather(bf16[4,512]{1,0:T(4,128)(2,1)} %param.16), channel_id=1, replica_groups=mesh['dp'=4,'kv'=4,'tp'=2] {'kv','tp'}, dimensions={1}, use_global_device_ids=true | all-gather | bytes 36864 | tf_op jit(solution)/shard_map/all_gather | solution.py:43
  23.4 0.8 fusion.13
  24.4 3.0 %fusion.35 = f32[4,2048]{1,0:T(4,128)S(1)} fusion(bf16[1024,2048]{1,0:T(8,128)(2,1)} %param.20, bf16[4,4096]{1,0:T(4,128)(2,1)S(1)} %fusion.13, s32[]{:T(128)S(6)} %select_n.24), kind=kOutput, calls=%fused_computation.51 | convolution fusion | flops 16777216 | bytes 4235268 | tf_op jit(solution)/shard_map/dot_general | solution.py:54
  27.4 0.4 fusion.37
  27.7 0.4 fusion.39
  28.1 0.7 pad_maximum_fusion
  28.9 0.2 fusion.5
  29.1 1.0 bitcast_add_fusion.1
  30.1 0.6 dynamic-slice
  30.7 33.5 %all-reduce.3.cloned.1.call-done = f32[4,4096]{1,0:T(4,128)} async-done(((f32[4,4096]{1,0:T(4,128)}), f32[4,4096]{1,0:T(4,128)}) %all-reduce.3.cloned.1.call-update) | async-done | bytes 65552
  64.2 1.5 dynamic-slice_reduce_fusion
  65.8 1.5 fusion.60
  67.2 1.0 fusion.6
  68.2 0.8 multiply_reduce_fusion.1
  69.1 13.1 %all-gather.1 = bf16[4,1,2048]{2,1,0:T(2,128)(2,1)S(1)} all-gather(bf16[1,1,2048]{2,1,0:T(2,128)(2,1)S(1)} %reshape.210), channel_id=1, replica_groups=mesh['dp'=4,'kv'=4,'tp'=2] {'kv'}, dimensions={0}, use_global_device_ids=true | all-gather | bytes 20480 | tf_op jit(solution)/shard_map/all_gather | solution.py:93
  82.3 2.8 %convolution_convert_fusion = bf16[4,1024]{1,0:T(4,128)(2,1)S(1)} fusion(bf16[2048,1024]{1,0:T(8,128)(2,1)} %param.28, bf16[4,1,2048]{2,1,0:T(2,128)(2,1)S(1)} %all-gather.1), kind=kOutput, calls=%fused_computation.4 | convolution fusion | flops 16781312 | bytes 4218880 | tf_op jit(solution)/shard_map/dot_general | solution.py:92
  85.1 14.0 %all-gather = bf16[4,8192]{1,0:T(4,128)(2,1)S(1)} all-gather(bf16[4,1024]{1,0:T(4,128)(2,1)S(1)} %convolution_convert_fusion), channel_id=2, replica_groups=mesh['dp'=4,'kv'=4,'tp'=2] {'kv','tp'}, dimensions={1}, use_global_device_ids=true | all-gather | bytes 73728 | tf_op jit(solution)/shard_map/all_gather | solution.py:98
  99.2 0.2 reduce_sum.54
  99.6 12.9 %convolution_bitcast_fusion = f32[4096,4]{0,1:T(4,128)S(1)} fusion(bf16[2048,4096]{1,0:T(8,128)(2,1)} %param.31, bf16[4096,2048]{1,0:T(8,128)(2,1)} %param.30, bf16[4,4096]{1,0:T(4,128)(2,1)S(1)} %get-tuple-element.9, f32[4096]{0:T(1024)S(1)} %copy-done.3, f32[4]{0:T(128)S(1)} %add_rsqrt_fusion), kind=kOutput, calls=%fused_computation | convolution fusion | flops 134307840 | bytes 33669136 | tf_op jit(solution)/shard_map/dot_general | solution.py:110
  112.5 2.0 %copy.22 = f32[4096,4]{1,0:T(8,128)} copy(f32[4096,4]{0,1:T(4,128)S(1)} %convolution_bitcast_fusion) | data formatting | bytes 131072
  114.5 1.3 multiply_add_fusion
  115.8 34.6 %reduce-scatter.4.cloned.1.call-done = f32[512,4]{1,0:T(8,128)} async-done(((f32[4096,4]{1,0:T(8,128)}), f32[512,4]{1,0:T(8,128)}) %reduce-scatter.4.cloned.1.call-update) | async-done | bytes 8208
  150.4 1.1 copy.23
  151.5 0.6 fusion.30
  (38 shorter events, 0.8 us)
Async XLA Ops:
  7.2 20.2 %copy-start = (bf16[1024,1024]{1,0:T(8,128)(2,1)S(1)}, bf16[1024,1024]{1,0:T(8,128)(2,1)}, u32[]{:S(2)}) copy-start(bf16[1024,1024]{1,0:T(8,128)(2,1)} %param.19) | copy-start | bytes 6291460
  7.2 57.1 %all-reduce.3.cloned.1.call-start = ((), (), s32[]{:S(2)}) async-start(), calls=%async_computation.2 | async-start | bytes 131072
  24.3 3.5 %copy-start.2 = (bf16[1024,1024]{1,0:T(8,128)(2,1)S(1)}, bf16[1024,1024]{1,0:T(8,128)(2,1)}, u32[]{:S(2)}) copy-start(bf16[1024,1024]{1,0:T(8,128)(2,1)} %param.18) | copy-start | bytes 6291460
  24.3 4.6 %copy-start.6 = (bf16[4096,16]{0,1:T(8,128)(2,1)S(1)}, bf16[4096,16]{0,1:T(8,128)(2,1)}, u32[]{:S(2)}) copy-start(bf16[4096,16]{0,1:T(8,128)(2,1)} %param.21) | copy-start | bytes 393220
  24.3 4.6 %copy-start.7 = (f32[16]{0:T(128)S(1)}, f32[16]{0:T(128)}, u32[]{:S(2)}) copy-start(f32[16]{0:T(128)} %param.23) | copy-start | bytes 196
  24.3 4.7 %copy-start.8 = (f32[1,8]{1,0:T(1,128)S(1)}, f32[1,8]{1,0:T(1,128)}, u32[]{:S(2)}) copy-start(f32[1,8]{1,0:T(1,128)} %param.27) | copy-start | bytes 100
  24.3 4.7 %copy-start.9 = (f32[16]{0:T(128)S(1)}, f32[16]{0:T(128)}, u32[]{:S(2)}) copy-start(f32[16]{0:T(128)} %param.24) | copy-start | bytes 196
  24.3 5.8 %copy-start.10 = (u32[32]{0:T(128)S(1)}, u32[32]{0:T(128)}, u32[]{:S(2)}) copy-start(u32[32]{0:T(128)} %constant.44) | copy-start | bytes 388
  24.3 42.9 %copy-start.1 = (f32[1,8,256,128]{3,2,1,0:T(8,128)S(1)}, f32[1,8,256,128]{3,2,1,0:T(8,128)}, u32[]{:S(2)}) copy-start(f32[1,8,256,128]{3,2,1,0:T(8,128)} %param.25) | copy-start | bytes 3145732
  24.3 43.9 %copy-start.4 = (f32[1,8,128]{2,1,0:T(8,128)S(1)}, f32[1,8,128]{2,1,0:T(8,128)}, u32[]{:S(2)}) copy-start(f32[1,8,128]{2,1,0:T(8,128)} %param.26) | copy-start | bytes 12292
  27.7 71.8 %copy-start.3 = (f32[4096]{0:T(1024)S(1)}, f32[4096]{0:T(1024)}, u32[]{:S(2)}) copy-start(f32[4096]{0:T(1024)} %param.29) | copy-start | bytes 49156
  28.8 121.6 %reduce-scatter.4.cloned.1.call-start = ((), (), s32[]{:S(2)}) async-start(), calls=%async_computation.1 | async-start | bytes 2359296
  30.1 82.4 %copy-start.5 = (f32[1,8]{1,0:T(1,128)}, f32[1,8]{1,0:T(1,128)S(1)}, u32[]{:S(2)}) copy-start(f32[1,8]{1,0:T(1,128)S(1)} %get-tuple-element.7) | copy-start | bytes 100
Sparse Core Ops, SparseCore 0:
  28.9 35.2 all-reduce.2
  114.6 35.7 reduce-scatter.3
where the time goes:
time: 159 us
  waiting for transfers between devices  68.2 us (43%)
  blocking collectives  43.2 us (27%)
  matrix products  21.6 us (14%)
  between operations  14.3 us (9%)
  other arithmetic  6.27 us (4%)
  local copies, waits for them, and re-layouts  5.36 us (3%)
    unnamed x4, waiting for transfers between devices  68.2 us
    all_gather x1, blocking collectives, on_device(): whole_rows = lax.all_gather(tokens, ('kv', 'tp'), axis=1, tiled=True)  16.1 us
    all_gather x1, blocking collectives, on_device(): lax.all_gather(partial_value.astype(jnp.bfloat16)[:, None, :], ('kv', 'tp...  14 us
    all_gather x1, blocking collectives, on_device(): lax.all_gather(cell_out, 'kv', axis=0, tiled=True)  13.1 us
    dot_general x1, matrix products, on_device(): lax.dot_general(w_down, activation, (((0,), (1,)), ((), ())), preferred_e...  12.9 us
    unnamed x27, local copies, waits for them, and re-layouts  3.77 us
  transfers between devices with their start and end apart: 2, of which 2 were waited for; matrix products, arithmetic and copies ran while one was open for 2% of the time, Pallas kernels for 0%

commit v1 on v0

--- a/solution.py
+++ b/solution.py
@@ -1,10 +1,16 @@
+import functools
+
 import jax
 import jax.numpy as jnp
 from jax import lax
+from jax.experimental import pallas as pl
+from jax.experimental.pallas import tpu as pltpu
 from jax.sharding import PartitionSpec as P
 
-DV = 256
-DQK = 128
+MESH = pl.DeviceIdType.MESH
+F32 = jnp.float32
+BF16 = jnp.bfloat16
+LANES = 128
 
 
 norm_eps = 1e-06
@@ -34,6 +40,7 @@
     w_up,
     w_down,
 ):
+    DV, DQK = memory.shape[2:]
     kv_count = lax.axis_size("kv")
     tp_count = lax.axis_size("tp")
     kv_index = lax.axis_index("kv")
@@ -121,6 +128,423 @@
     return (new_tokens, new_memory, new_normalizer, new_stabilizer)
 
 
+def fused_cell(
+    n_kv,
+    n_tp,
+    tok_h, mixg_h, wq_h, wk_h, wv_h, wig_h, wfg_h, ib_h, fb_h,
+    mem_h, nrm_h, stb_h, wo_h, mlpg_h, wup_h, wdn_h,
+    otok, omem_h, onrm, ostb,
+    tok, tokall, mixg, wq, wk, wv, wig, wfg, ib, fb,
+    mem, membf, newmem, nrm, stb, wo, mlpg, wup, wdn,
+    snd, rcv, cell_own, cell_all, y_own, y_all, mid, acc, act, stage, land,
+    small_sem, w_sem, up_sem, out_sem,
+    tok_s, tok_r, rs_s, rs_r, cell_s, cell_r, y_s, y_r, dn_s, dn_r,
+):
+    dp = lax.axis_index("dp")
+    kv = lax.axis_index("kv")
+    tp = lax.axis_index("tp")
+    n_all = n_kv * n_tp
+    g = kv * n_tp + tp
+    batch, thin = tok.shape
+    span = wq.shape[0]
+    heads, dv, dqk = mem.shape
+    width = tokall.shape[0] * thin
+    halves = dv // LANES
+
+    def peer_of(offset):
+        other = (g + offset) % n_all
+        return other, (dp, other // n_tp, other % n_tp)
+
+    barrier = pltpu.get_barrier_semaphore()
+    for o in range(1, n_all):
+        pl.semaphore_signal(barrier, inc=1, device_id=peer_of(o)[1], device_id_type=MESH)
+
+    own_span = pl.ds(pl.multiple_of(kv * span, span), span)
+    smalls = [
+        (tok_h, tok), (mixg_h, mixg), (wig_h.at[own_span], wig), (wfg_h.at[own_span], wfg),
+        (ib_h, ib), (fb_h, fb), (nrm_h.at[0], nrm), (stb_h, stb), (mlpg_h, mlpg),
+    ]
+    small = [pltpu.make_async_copy(a, b, small_sem.at[i]) for i, (a, b) in enumerate(smalls)]
+    bigs = [(wq_h, wq), (wk_h, wk), (wv_h, wv), (mem_h.at[0], mem), (wo_h, wo), (wdn_h, wdn)]
+    big = [pltpu.make_async_copy(a, b, w_sem.at[i]) for i, (a, b) in enumerate(bigs)]
+    for c in small:
+        c.start()
+    for c in big[:5]:
+        c.start()
+
+    def up_rows(i):
+        off = i + (i // 2) * (5 - 2 * i) if n_kv == 4 else i
+        j = (kv + off) % n_kv
+        return j, pl.ds(pl.multiple_of(j * span, span), span)
+
+    def up_copy(i):
+        j, rows = up_rows(i)
+        return pltpu.make_async_copy(wup_h.at[rows], wup.at[rows], up_sem.at[j])
+
+    small[0].wait()
+    pl.semaphore_wait(barrier, n_all - 1)
+
+    def tok_copy(o):
+        return pltpu.make_async_remote_copy(
+            src_ref=tok, dst_ref=tokall.at[g], send_sem=tok_s.at[o], recv_sem=tok_r.at[g],
+            device_id=peer_of(o)[1], device_id_type=MESH)
+
+    def tok_wait(src):
+        pltpu.make_async_remote_copy(
+            src_ref=tok, dst_ref=tokall.at[src], send_sem=tok_s.at[0], recv_sem=tok_r.at[src],
+            device_id=peer_of(1)[1], device_id_type=MESH).wait_recv()
+
+    mate = [(kv * n_tp + (tp + t) % n_tp) for t in range(1, n_tp)]
+    for src in mate:
+        pltpu.make_async_remote_copy(
+            src_ref=tok, dst_ref=tokall.at[g], send_sem=tok_s.at[src], recv_sem=tok_r.at[g],
+            device_id=(dp, kv, src % n_tp), device_id_type=MESH).start()
+    tokall[g] = tok[...]
+
+    def far_tok(o, t):
+        to = (kv + o) % n_kv
+        other = to * n_tp + (tp + t) % n_tp
+        return other, pltpu.make_async_remote_copy(
+            src_ref=tok, dst_ref=tokall.at[g], send_sem=tok_s.at[other], recv_sem=tok_r.at[g],
+            device_id=(dp, to, (tp + t) % n_tp), device_id_type=MESH)
+
+    for o in range(1, n_kv):
+        for t in range(n_tp):
+            far_tok(o, t)[1].start()
+
+    snd[:, heads : 2 * heads, :] = jnp.zeros((n_kv, heads, LANES), F32)
+    for src in mate:
+        tok_wait(src)
+    for c in small[1:]:
+        c.wait()
+
+    def chunk(t):
+        return tokall[kv * n_tp + t].astype(F32)
+
+    raw = jnp.concatenate([chunk(t) for t in range(n_tp)], axis=1)
+    x = (raw * mixg[:, own_span]).astype(BF16)
+    squares = jnp.sum(raw * raw, axis=1, keepdims=True)
+    snd[:, heads + 2, :] = jnp.broadcast_to(squares, (n_kv, LANES))
+    gate_count = wig.shape[1]
+    snd[:, heads, :gate_count] = jnp.dot(x, wig[...], preferred_element_type=F32)
+    snd[:, heads + 1, :gate_count] = jnp.dot(x, wfg[...], preferred_element_type=F32)
+
+    pieces = [(0, 2 * heads), (2 * heads, heads), (3 * heads, halves * heads)]
+
+    def rs_copy(o, p):
+        first, size = pieces[p]
+        to = (kv + o) % n_kv
+        return pltpu.make_async_remote_copy(
+            src_ref=snd.at[to, pl.ds(first, size)],
+            dst_ref=rcv.at[o, pl.ds(first, size)],
+            send_sem=rs_s.at[o, p], recv_sem=rs_r.at[o, p],
+            device_id=(dp, to, tp), device_id_type=MESH)
+
+    far_first = sorted(range(1, n_kv), key=lambda o: -min(o, n_kv - o))
+    big[0].wait()
+    q_part = jnp.dot(x, wq[...], preferred_element_type=F32)
+    for h in range(heads):
+        snd[:, h, :] = q_part[:, h * dqk : (h + 1) * dqk]
+    for o in far_first:
+        rs_copy(o, 0).start()
+    big[1].wait()
+    up_copy(0).start()
+    up_copy(1).start()
+    k_part = jnp.dot(x, wk[...], preferred_element_type=F32)
+    for h in range(heads):
+        snd[:, 2 * heads + h, :] = k_part[:, h * dqk : (h + 1) * dqk]
+    for o in far_first:
+        rs_copy(o, 1).start()
+    big[2].wait()
+    for i in range(2, n_kv):
+        up_copy(i).start()
+    v_part = jnp.dot(x, wv[...], preferred_element_type=F32)
+    for h in range(heads):
+        for s in range(halves):
+            at = h * dv + s * LANES
+            snd[:, (3 + s) * heads + h, :] = v_part[:, at : at + LANES]
+    for o in far_first:
+        rs_copy(o, 2).start()
+    big[5].start()
+    big[3].wait()
+    membf[...] = mem[...].astype(BF16).reshape(heads * dv, dqk)
+
+    lane = lax.broadcasted_iota(jnp.int32, (heads, LANES), 1)
+    sub = lax.broadcasted_iota(jnp.int32, (heads, LANES), 0)
+    own_head = lane == sub + tp * heads
+
+    def column(row):
+        wide = jnp.pad(row, ((0, 0), (0, LANES - row.shape[1]))) if row.shape[1] < LANES else row
+        return jnp.sum(jnp.where(own_head, jnp.broadcast_to(wide, own_head.shape), 0.0), axis=1, keepdims=True)
+
+    def joined(p):
+        first, size = pieces[p]
+        total = snd[kv, first : first + size, :]
+        for o in range(1, n_kv):
+            rs_copy(o, p).wait_recv()
+            total = total + rcv[o, first : first + size, :]
+        return total
+
+    part = joined(0)
+    scale = lax.rsqrt(part[heads + 2 : heads + 3] * (1.0 / width) + norm_eps)
+    q = part[:heads] * scale * dqk**-0.5
+    gate_i = column(part[heads : heads + 1] * scale) + column(ib[...])
+    gate_f = column(part[heads + 1 : heads + 2] * scale) + column(fb[...])
+    log_forget = jnp.minimum(gate_f, 0.0) - jnp.log1p(jnp.exp(-jnp.abs(gate_f)))
+    stab_wide = jnp.broadcast_to(stb[...], (heads, heads))
+    eye = (lax.broadcasted_iota(jnp.int32, (heads, heads), 0)
+           == lax.broadcasted_iota(jnp.int32, (heads, heads), 1))
+    stab = jnp.sum(jnp.where(eye, stab_wide, 0.0), axis=1, keepdims=True)
+    carried = log_forget + stab
+    new_stab = jnp.maximum(carried, gate_i)
+    keep = jnp.exp(carried - new_stab)
+    fresh = jnp.exp(gate_i - new_stab)
+    ostb[...] = jnp.sum(jnp.where(eye, jnp.broadcast_to(new_stab, (heads, heads)), 0.0), axis=0, keepdims=True)
+    norm_dot = jnp.sum(nrm[...] * q, axis=1, keepdims=True)
+    q_hi = q.astype(BF16)
+    q_lo = (q - q_hi.astype(F32)).astype(BF16)
+    wide_recall = lax.dot_general(
+        jnp.concatenate([q_hi, q_lo], axis=0), membf[...], (((1,), (1,)), ((), ())),
+        preferred_element_type=F32)
+    wide_recall = wide_recall[:heads] + wide_recall[heads:]
+    row_id = lax.broadcasted_iota(jnp.int32, (heads, dv), 0)
+    recall = jnp.zeros((heads, dv), F32)
+    for h in range(heads):
+        recall = jnp.where(row_id == h, wide_recall[:, h * dv : (h + 1) * dv], recall)
+    k = joined(1) * scale
+    match = jnp.sum(q * k, axis=1, keepdims=True)
+    denominator = keep * norm_dot + fresh * match
+    floor_value = jnp.maximum(jnp.abs(denominator), jnp.exp(-new_stab))
+    v_rows = joined(2)
+    v = jnp.concatenate([v_rows[s * heads : (s + 1) * heads] * scale for s in range(halves)], axis=1)
+    cell = (keep * recall + (fresh * match) * v) / floor_value
+    cell_own[...] = cell
+
+    def cell_copy(o):
+        to = (kv + o) % n_kv
+        return pltpu.make_async_remote_copy(
+            src_ref=cell_own, dst_ref=cell_all.at[kv], send_sem=cell_s.at[o], recv_sem=cell_r.at[o],
+            device_id=(dp, to, tp), device_id_type=MESH)
+
+    for o in far_first:
+        cell_copy(o).start()
+    cell_all[kv] = cell
+    onrm[0] = keep * nrm[...] + fresh * k
+    fresh_v = fresh * v
+    fresh_vt = fresh_v.T
+    for h in range(heads):
+        newmem[h] = keep[h : h + 1] * mem[h] + fresh_vt[:, h : h + 1] * k[h : h + 1]
+    out_mem = pltpu.make_async_copy(newmem, omem_h.at[0], out_sem.at[0])
+    out_mem.start()
+    big[4].wait()
+    for o in range(1, n_kv):
+        src = (kv + n_kv - o) % n_kv
+        pltpu.make_async_remote_copy(
+            src_ref=cell_own, dst_ref=cell_all.at[src], send_sem=cell_s.at[o], recv_sem=cell_r.at[o],
+            device_id=(dp, src, tp), device_id_type=MESH).wait_recv()
+    rows = jnp.concatenate([cell_all[:, h, :] for h in range(heads)], axis=1).astype(BF16)
+    y = jnp.dot(rows, wo[...], preferred_element_type=F32).astype(BF16)
+    y_own[...] = y
+
+    def y_copy(o, t):
+        to = (kv + o) % n_kv
+        to_tp = (tp + t) % n_tp
+        return pltpu.make_async_remote_copy(
+            src_ref=y_own, dst_ref=y_all.at[g], send_sem=y_s.at[to * n_tp + to_tp], recv_sem=y_r.at[g],
+            device_id=(dp, to, to_tp), device_id_type=MESH)
+
+    for o in far_first + [0]:
+        for t in range(n_tp):
+            if o or t:
+                y_copy(o, t).start()
+    y_all[g] = y
+    for o in range(1, n_kv):
+        for t in range(n_tp):
+            tok_wait(((kv + o) % n_kv) * n_tp + (tp + t) % n_tp)
+
+    def y_wait(src):
+        pltpu.make_async_remote_copy(
+            src_ref=y_own, dst_ref=y_all.at[src], send_sem=y_s.at[0], recv_sem=y_r.at[src],
+            device_id=peer_of(1)[1], device_id_type=MESH).wait_recv()
+
+    def up_step(i, square_sum):
+        j, span_rows = up_rows(i)
+        up_copy(i).wait()
+        for t in range(1, n_tp):
+            y_wait(j * n_tp + (tp + t) % n_tp)
+
+        @pl.when(i > 0)
+        def _():
+            y_wait(j * n_tp + tp)
+
+        base = jnp.concatenate([tokall[j * n_tp + t].astype(F32) for t in range(n_tp)], axis=1)
+        for t in range(n_tp):
+            base = base + y_all[j * n_tp + t].astype(F32)
+        m = base.astype(BF16).astype(F32)
+        mid[j] = m
+        mixed = (m * mlpg[:, span_rows]).astype(BF16)
+        part = jnp.dot(mixed, wup[span_rows, :], preferred_element_type=F32)
+
+        @pl.when(i == 0)
+        def _():
+            acc[...] = part
+
+        @pl.when(i > 0)
+        def _():
+            acc[...] += part
+
+        return square_sum + jnp.sum(m * m, axis=1, keepdims=True)
+
+    square_sum = lax.fori_loop(0, n_kv, up_step, jnp.zeros((batch, 1), F32))
+    scale2 = lax.rsqrt(square_sum * (1.0 / width) + norm_eps)
+    up = jnp.maximum(acc[...] * scale2, 0.0)
+    act[...] = (up * up).astype(BF16)
+    big[5].wait()
+
+    def dn_copy(o):
+        return pltpu.make_async_remote_copy(
+            src_ref=stage.at[o], dst_ref=land.at[o], send_sem=dn_s.at[o], recv_sem=dn_r.at[o],
+            device_id=peer_of(o)[1], device_id_type=MESH)
+
+    def down_step(i, carry):
+        o = 1 + (i + n_all // 2 - 1) % (n_all - 1) + (i // (n_all - 1)) * (n_all - 1 - (n_all // 2 - 1))
+        o = o % n_all
+        other, _ = peer_of(o)
+        cols = pl.ds(pl.multiple_of(other * thin, thin), thin)
+        stage[o] = jnp.dot(act[...], wdn[:, cols], preferred_element_type=F32)
+
+        @pl.when(i < n_all - 1)
+        def _():
+            dn_copy(o).start()
+
+        return carry
+
+    lax.fori_loop(0, n_all, down_step, 0)
+    total = mid[kv, :, pl.ds(pl.multiple_of(tp * thin, thin), thin)] + stage[0]
+    for o in range(1, n_all):
+        dn_copy(o).wait_recv()
+        total = total + land[o]
+    otok[...] = total.astype(BF16)
+
+    for src in mate:
+        pltpu.make_async_remote_copy(
+            src_ref=tok, dst_ref=tokall.at[g], send_sem=tok_s.at[src], recv_sem=tok_r.at[g],
+            device_id=(dp, kv, src % n_tp), device_id_type=MESH).wait_send()
+    for o in range(n_kv):
+        for t in range(n_tp):
+            if o:
+                far_tok(o, t)[1].wait_send()
+            if o or t:
+                y_copy(o, t).wait_send()
+        if o:
+            for p in range(len(pieces)):
+                rs_copy(o, p).wait_send()
+            cell_copy(o).wait_send()
+    for o in range(1, n_all):
+        dn_copy(o).wait_send()
+    out_mem.wait()
+
+
+def fits_fused(tokens, w_query, w_value, memory, w_output, w_up, w_down, n_kv, n_tp):
+    own_rows, heads, dv, dqk = memory.shape
+    batch, thin = tokens.shape
+    span = w_query.shape[0]
+    held = 2 * (2 * w_query.size + w_value.size + w_output.size + w_up.size + w_down.size)
+    held += 10 * memory.size
+    return (
+        own_rows == 1 and batch == n_kv and heads == 8 and dqk == LANES and dv % LANES == 0
+        and thin % LANES == 0 and span == n_tp * thin and n_kv >= 2 and n_tp >= 2
+        and w_output.shape[1] == span and held < 52 * 2**20
+    )
+
+
+def fused_on_device(
+    tokens, mix_gain, w_query, w_key, w_value, w_igate, w_fgate, igate_bias, fgate_bias,
+    memory, normalizer, stabilizer, w_output, mlp_gain, w_up, w_down,
+):
+    n_kv = lax.axis_size("kv")
+    n_tp = lax.axis_size("tp")
+    n_all = n_kv * n_tp
+    batch, thin = tokens.shape
+    _, heads, dv, dqk = memory.shape
+    span = w_query.shape[0]
+    width = n_all * thin
+    halves = dv // LANES
+    groups = (3 + halves) * heads
+    hidden = w_up.shape[1]
+    any_spec = pl.BlockSpec(memory_space=pl.ANY)
+    vmem_spec = pl.BlockSpec(memory_space=pltpu.VMEM)
+    vm = pltpu.VMEM
+    dma = pltpu.SemaphoreType.DMA
+    scratch = [
+        vm((batch, thin), BF16),
+        vm((n_all, batch, thin), BF16),
+        vm((1, width), F32),
+        vm(w_query.shape, BF16),
+        vm(w_key.shape, BF16),
+        vm(w_value.shape, BF16),
+        vm((span, w_igate.shape[1]), BF16),
+        vm((span, w_fgate.shape[1]), BF16),
+        vm((1, igate_bias.shape[0]), F32),
+        vm((1, fgate_bias.shape[0]), F32),
+        vm((heads, dv, dqk), F32),
+        vm((heads * dv, dqk), BF16),
+        vm((heads, dv, dqk), F32),
+        vm((heads, dqk), F32),
+        vm((1, heads), F32),
+        vm(w_output.shape, BF16),
+        vm((1, width), F32),
+        vm(w_up.shape, BF16),
+        vm(w_down.shape, BF16),
+        vm((n_kv, groups, LANES), F32),
+        vm((n_kv, groups, LANES), F32),
+        vm((heads, dv), F32),
+        vm((n_kv, heads, dv), F32),
+        vm((batch, span), BF16),
+        vm((n_all, batch, span), BF16),
+        vm((n_kv, batch, span), F32),
+        vm((batch, hidden), F32),
+        vm((batch, hidden), BF16),
+        vm((n_all, batch, thin), F32),
+        vm((n_all, batch, thin), F32),
+        dma((9,)), dma((6,)), dma((n_kv,)), dma((1,)),
+        dma((n_all,)), dma((n_all,)),
+        dma((n_kv, 3)), dma((n_kv, 3)),
+        dma((n_kv,)), dma((n_kv,)),
+        dma((n_all,)), dma((n_all,)),
+        dma((n_all,)), dma((n_all,)),
+    ]
+    return pl.pallas_call(
+        functools.partial(fused_cell, n_kv, n_tp),
+        out_shape=(
+            jax.ShapeDtypeStruct(tokens.shape, BF16),
+            jax.ShapeDtypeStruct(memory.shape, F32),
+            jax.ShapeDtypeStruct(normalizer.shape, F32),
+            jax.ShapeDtypeStruct(stabilizer.shape, F32),
+        ),
+        in_specs=[any_spec] * 16,
+        out_specs=(vmem_spec, any_spec, vmem_spec, vmem_spec),
+        scratch_shapes=scratch,
+        compiler_params=pltpu.CompilerParams(
+            collective_id=0, has_side_effects=True, vmem_limit_bytes=60 * 2**20
+        ),
+        name="fused_cell",
+    )(
+        tokens, mix_gain.reshape(1, -1), w_query, w_key, w_value, w_igate, w_fgate,
+        igate_bias.reshape(1, -1), fgate_bias.reshape(1, -1), memory, normalizer, stabilizer,
+        w_output, mlp_gain.reshape(1, -1), w_up, w_down,
+    )
+
+
+def routed(*arrays):
+    tokens, w_query, w_value, memory = arrays[0], arrays[2], arrays[4], arrays[9]
+    w_output, w_up, w_down = arrays[12], arrays[14], arrays[15]
+    n_kv, n_tp = lax.axis_size("kv"), lax.axis_size("tp")
+    if fits_fused(tokens, w_query, w_value, memory, w_output, w_up, w_down, n_kv, n_tp):
+        return fused_on_device(*arrays)
+    return on_device(*arrays)
+
+
 def solution(mesh):
     in_specs = (
         P("dp", ("kv", "tp")),
@@ -147,5 +571,5 @@
         P(("dp", "kv"), "tp"),
     )
     return jax.shard_map(
-        on_device, mesh=mesh, in_specs=in_specs, out_specs=out_specs, check_vma=False
-    )
+        routed, mesh=mesh, in_specs=in_specs, out_specs=out_specs, check_vma=False
+    )

time: 159 us -> 40.4 us (0.25)
  waiting for transfers between devices: 68.2 us -> 0 us
  blocking collectives: 43.2 us -> 0 us
  Pallas kernels: 0 us -> 29.1 us
  matrix products: 21.6 us -> 0 us
  between operations: 14.3 us -> 0.64 us
  other arithmetic: 6.27 us -> 0 us
  local copies, waits for them, and re-layouts: 5.36 us -> 10.4 us
    unnamed x4 -> x0, waiting for transfers between devices: 68.2 us -> none
    all_gather x3 -> x0, blocking collectives: 43.2 us -> none  [the longest x1 16.1 us: on_device(): whole_rows = lax.all_gather(tokens, ('kv', 'tp'), axis=1, tiled=True)]
    pallas_call x0 -> x1, Pallas kernels: none -> 29.1 us  [fused_on_device(): pl.pallas_call(functools.partial(fused_cell, n_kv, n_tp), out_shape=(jax....]
    dot_general x8 -> x0, matrix products: 21.6 us -> none  [the longest x1 12.9 us: on_device(): lax.dot_general(w_down, activation, (((0,), (1,)), ((), ())), preferred_e...]
    unnamed x27 -> x6, local copies, waits for them, and re-layouts: 3.77 us -> 10.4 us
  transfers between devices with their start and end apart: 2 -> 0, of which waited for: 2 -> 0; matrix products, arithmetic and copies ran while one was open for 2% -> 0% of each run, Pallas kernels for 0% -> 0%
where the time goes in v1:
time: 40.4 us; the launch traced here: 40.1 us
  Pallas kernels  29.1 us (72%)
  local copies, waits for them, and re-layouts  10.4 us (26%)
  between operations  0.64 us (2%)
    pallas_call x1, Pallas kernels, fused_on_device(): pl.pallas_call(functools.partial(fused_cell, n_kv, n_tp), out_shape=(jax....  29.1 us
    unnamed x6, local copies, waits for them, and re-layouts  10.4 us

profile of v1, /device:TPU:0, one launch (start us, length us, event | category | flops | bytes accessed | tf_op | source)
XLA Modules:
  0.0 40.1 jit_solution(13452208339258195849)
XLA Ops:
  0.6 2.2 %copy.20.wig_h = bf16[4096,16]{1,0:T(8,128)(2,1)} copy(bf16[4096,16]{0,1:T(8,128)(2,1)} %param.21) | data formatting | bytes 262144 | tf_op args[5]
  2.9 2.2 %copy.21.wfg_h = bf16[4096,16]{1,0:T(8,128)(2,1)} copy(bf16[4096,16]{0,1:T(8,128)(2,1)} %param.22) | data formatting | bytes 262144 | tf_op args[6]
  5.1 29.1 %fused_cell.1 = (bf16[4,512]{1,0:T(4,128)(2,1)}, f32[1,8,256,128]{3,2,1,0:T(8,128)}, f32[1,8,128]{2,1,0:T(8,128)}, f32[1,8]{1,0:T(1,128)}) custom-call(bf16[4,512]{1,0:T(4,128)(2,1)} %tok_h.1, f32[1,4096]{1,0:T(1,128)} %bitcast.4, bf16[1024,1024]{1,0:T(8,128)(2,1)} %wq_h.1, bf16[1024,1024]{1,0:T(8,128)(2,1)} %wk_h.1, bf16[1024,2048]{1,0:T(8,128)(2,1)} %wv_h.1, ...), custom_call_target="tpu_custom_call" | custom-call | tf_op jit(solution)/shard_map/fused_cell/pallas_call | solution.py:517
  34.2 1.3 %copy.26 = bf16[4,512]{1,0:T(4,128)(2,1)} copy(bf16[4,512]{1,0:T(4,128)(2,1)} %get-tuple-element.8) | data formatting | bytes 8192
  35.5 2.3 %copy.27 = f32[1,8,256,128]{3,2,1,0:T(8,128)} copy(f32[1,8,256,128]{3,2,1,0:T(8,128)} %get-tuple-element.9) | data formatting | bytes 2097152
  37.8 1.3 %copy.28 = f32[1,8,128]{2,1,0:T(8,128)} copy(f32[1,8,128]{2,1,0:T(8,128)} %get-tuple-element.10) | data formatting | bytes 8192
  39.1 1.1 %copy.29 = f32[1,8]{1,0:T(1,128)} copy(f32[1,8]{1,0:T(1,128)} %get-tuple-element.11) | data formatting | bytes 64

commit v2 on v1

--- a/solution.py
+++ b/solution.py
@@ -133,11 +133,11 @@
     n_tp,
     tok_h, mixg_h, wq_h, wk_h, wv_h, wig_h, wfg_h, ib_h, fb_h,
     mem_h, nrm_h, stb_h, wo_h, mlpg_h, wup_h, wdn_h,
-    otok, omem_h, onrm, ostb,
+    otok, newmem, onrm, ostb,
     tok, tokall, mixg, wq, wk, wv, wig, wfg, ib, fb,
-    mem, membf, newmem, nrm, stb, wo, mlpg, wup, wdn,
+    mem, membf, nrm, stb, wo, mlpg, wup, wdn,
     snd, rcv, cell_own, cell_all, y_own, y_all, mid, acc, act, stage, land,
-    small_sem, w_sem, up_sem, out_sem,
+    small_sem, w_sem, up_sem,
     tok_s, tok_r, rs_s, rs_r, cell_s, cell_r, y_s, y_r, dn_s, dn_r,
 ):
     dp = lax.axis_index("dp")
@@ -161,7 +161,7 @@
 
     own_span = pl.ds(pl.multiple_of(kv * span, span), span)
     smalls = [
-        (tok_h, tok), (mixg_h, mixg), (wig_h.at[own_span], wig), (wfg_h.at[own_span], wfg),
+        (tok_h, tok), (mixg_h, mixg), (wig_h.at[:, own_span], wig), (wfg_h.at[:, own_span], wfg),
         (ib_h, ib), (fb_h, fb), (nrm_h.at[0], nrm), (stb_h, stb), (mlpg_h, mlpg),
     ]
     small = [pltpu.make_async_copy(a, b, small_sem.at[i]) for i, (a, b) in enumerate(smalls)]
@@ -225,9 +225,10 @@
     x = (raw * mixg[:, own_span]).astype(BF16)
     squares = jnp.sum(raw * raw, axis=1, keepdims=True)
     snd[:, heads + 2, :] = jnp.broadcast_to(squares, (n_kv, LANES))
-    gate_count = wig.shape[1]
-    snd[:, heads, :gate_count] = jnp.dot(x, wig[...], preferred_element_type=F32)
-    snd[:, heads + 1, :gate_count] = jnp.dot(x, wfg[...], preferred_element_type=F32)
+    gate_count = wig.shape[0]
+    last = (((1,), (1,)), ((), ()))
+    snd[:, heads, :gate_count] = lax.dot_general(x, wig[...], last, preferred_element_type=F32)
+    snd[:, heads + 1, :gate_count] = lax.dot_general(x, wfg[...], last, preferred_element_type=F32)
 
     pieces = [(0, 2 * heads), (2 * heads, heads), (3 * heads, halves * heads)]
 
@@ -333,9 +334,7 @@
     fresh_v = fresh * v
     fresh_vt = fresh_v.T
     for h in range(heads):
-        newmem[h] = keep[h : h + 1] * mem[h] + fresh_vt[:, h : h + 1] * k[h : h + 1]
-    out_mem = pltpu.make_async_copy(newmem, omem_h.at[0], out_sem.at[0])
-    out_mem.start()
+        newmem[0, h] = keep[h : h + 1] * mem[h] + fresh_vt[:, h : h + 1] * k[h : h + 1]
     big[4].wait()
     for o in range(1, n_kv):
         src = (kv + n_kv - o) % n_kv
@@ -442,7 +441,15 @@
             cell_copy(o).wait_send()
     for o in range(1, n_all):
         dn_copy(o).wait_send()
-    out_mem.wait()
+
+
+def hand_over(a, b, c, d, out_a, out_b, out_c, out_d, sems):
+    pairs = ((b, out_b), (a, out_a), (c, out_c), (d, out_d))
+    copies = [pltpu.make_async_copy(x, y, sems.at[i]) for i, (x, y) in enumerate(pairs)]
+    for c in copies:
+        c.start()
+    for c in copies:
+        c.wait()
 
 
 def fits_fused(tokens, w_query, w_value, memory, w_output, w_up, w_down, n_kv, n_tp):
@@ -472,7 +479,7 @@
     halves = dv // LANES
     groups = (3 + halves) * heads
     hidden = w_up.shape[1]
-    any_spec = pl.BlockSpec(memory_space=pl.ANY)
+    hbm_spec = pl.BlockSpec(memory_space=pltpu.HBM)
     vmem_spec = pl.BlockSpec(memory_space=pltpu.VMEM)
     vm = pltpu.VMEM
     dma = pltpu.SemaphoreType.DMA
@@ -483,13 +490,12 @@
         vm(w_query.shape, BF16),
         vm(w_key.shape, BF16),
         vm(w_value.shape, BF16),
-        vm((span, w_igate.shape[1]), BF16),
-        vm((span, w_fgate.shape[1]), BF16),
+        vm((w_igate.shape[1], span), BF16),
+        vm((w_fgate.shape[1], span), BF16),
         vm((1, igate_bias.shape[0]), F32),
         vm((1, fgate_bias.shape[0]), F32),
         vm((heads, dv, dqk), F32),
         vm((heads * dv, dqk), BF16),
-        vm((heads, dv, dqk), F32),
         vm((heads, dqk), F32),
         vm((1, heads), F32),
         vm(w_output.shape, BF16),
@@ -507,14 +513,20 @@
         vm((batch, hidden), BF16),
         vm((n_all, batch, thin), F32),
         vm((n_all, batch, thin), F32),
-        dma((9,)), dma((6,)), dma((n_kv,)), dma((1,)),
+        dma((9,)), dma((6,)), dma((n_kv,)),
         dma((n_all,)), dma((n_all,)),
         dma((n_kv, 3)), dma((n_kv, 3)),
         dma((n_kv,)), dma((n_kv,)),
         dma((n_all,)), dma((n_all,)),
         dma((n_all,)), dma((n_all,)),
     ]
-    return pl.pallas_call(
+    args = (
+        tokens, mix_gain.reshape(1, -1), w_query, w_key, w_value, w_igate.T, w_fgate.T,
+        igate_bias.reshape(1, -1), fgate_bias.reshape(1, -1), memory, normalizer, stabilizer,
+        w_output, mlp_gain.reshape(1, -1), w_up, w_down,
+    )
+    args = [pltpu.with_memory_space_constraint(a, pltpu.HBM) for a in args]
+    results = pl.pallas_call(
         functools.partial(fused_cell, n_kv, n_tp),
         out_shape=(
             jax.ShapeDtypeStruct(tokens.shape, BF16),
@@ -522,18 +534,23 @@
             jax.ShapeDtypeStruct(normalizer.shape, F32),
             jax.ShapeDtypeStruct(stabilizer.shape, F32),
         ),
-        in_specs=[any_spec] * 16,
-        out_specs=(vmem_spec, any_spec, vmem_spec, vmem_spec),
+        in_specs=[hbm_spec] * 16,
+        out_specs=(vmem_spec,) * 4,
         scratch_shapes=scratch,
         compiler_params=pltpu.CompilerParams(
-            collective_id=0, has_side_effects=True, vmem_limit_bytes=60 * 2**20
+            collective_id=0, has_side_effects=True, vmem_limit_bytes=52 * 2**20
         ),
         name="fused_cell",
-    )(
-        tokens, mix_gain.reshape(1, -1), w_query, w_key, w_value, w_igate, w_fgate,
-        igate_bias.reshape(1, -1), fgate_bias.reshape(1, -1), memory, normalizer, stabilizer,
-        w_output, mlp_gain.reshape(1, -1), w_up, w_down,
-    )
+    )(*args)
+    return pl.pallas_call(
+        hand_over,
+        out_shape=tuple(jax.ShapeDtypeStruct(r.shape, r.dtype) for r in results),
+        in_specs=[vmem_spec] * 4,
+        out_specs=(hbm_spec,) * 4,
+        scratch_shapes=[dma((4,))],
+        compiler_params=pltpu.CompilerParams(vmem_limit_bytes=2**20),
+        name="hand_over",
+    )(*results)
 
 
 def routed(*arrays):

time: 40.4 us -> 30.4 us (0.75)
  local copies, waits for them, and re-layouts: 10.4 us -> 0 us
  Pallas kernels: 29.1 us -> 29.6 us
    unnamed x6 -> x0, local copies, waits for them, and re-layouts: 10.4 us -> none
    pallas_call x0 -> x1, Pallas kernels: none -> 1.01 us  [fused_on_device(): pl.pallas_call(hand_over, out_shape=tuple((jax.ShapeDtypeStruct(r.shape,...]
    pallas_call x1, Pallas kernels: 29.1 us -> 28.6 us  [fused_on_device(): pl.pallas_call(functools.partial(fused_cell, n_kv, n_tp), out_shape=(jax....]
where the time goes in v2:
time: 30.4 us; the launch traced here: 30.2 us
  Pallas kernels  29.6 us (97%)
  between operations  0.65 us (2%)
    pallas_call x1, Pallas kernels, fused_on_device(): pl.pallas_call(functools.partial(fused_cell, n_kv, n_tp), out_shape=(jax....  28.6 us
    pallas_call x1, Pallas kernels, fused_on_device(): pl.pallas_call(hand_over, out_shape=tuple((jax.ShapeDtypeStruct(r.shape,...  1.01 us

profile of v2, /device:TPU:0, one launch (start us, length us, event | category | flops | bytes accessed | tf_op | source)
XLA Modules:
  0.0 30.2 jit_solution(6616449874710289699)
XLA Ops:
  0.6 28.6 %fused_cell.1 = (bf16[4,512]{1,0:T(4,128)(2,1)S(1)}, f32[1,8,256,128]{3,2,1,0:T(8,128)S(1)}, f32[1,8,128]{2,1,0:T(8,128)S(1)}, f32[1,8]{1,0:T(1,128)S(1)}) custom-call(bf16[4,512]{1,0:T(4,128)(2,1)} %tok_h.1, f32[1,4096]{1,0:T(1,128)} %bitcast.8, bf16[1024,1024]{1,0:T(8,128)(2,1)} %wq_h.1, bf16[1024,1024]{1,0:T(8,128)(2,1)} %wk_h.1, ...), custom_call_target="tpu_custom_call" | custom-call | tf_op jit(solution)/shard_map/fused_cell/pallas_call | solution.py:529
  29.2 1.0 %hand_over.1 = (bf16[4,512]{1,0:T(4,128)(2,1)}, f32[1,8,256,128]{3,2,1,0:T(8,128)}, f32[1,8,128]{2,1,0:T(8,128)}, f32[1,8]{1,0:T(1,128)}) custom-call(bf16[4,512]{1,0:T(4,128)(2,1)S(1)} %get-tuple-element.8.a, f32[1,8,256,128]{3,2,1,0:T(8,128)S(1)} %get-tuple-element.9.b, f32[1,8,128]{2,1,0:T(8,128)S(1)} %get-tuple-element.10.c, f32[1,8]{1,0:T(1,128)S(1)} %get-tuple-element.11.d), custom_call_target="tpu_custom_call" | custom-call | tf_op jit(solution)/shard_map/hand_over/pallas_call | solution.py:545

commit v3 on v2

--- a/solution.py
+++ b/solution.py
@@ -136,7 +136,7 @@
     otok, newmem, onrm, ostb,
     tok, tokall, mixg, wq, wk, wv, wig, wfg, ib, fb,
     mem, membf, nrm, stb, wo, mlpg, wup, wdn,
-    snd, rcv, cell_own, cell_all, y_own, y_all, mid, acc, act, stage, land,
+    snd, rcv, cell_own, cell_all, y_own, y_all, mid, act, stage, land,
     small_sem, w_sem, up_sem,
     tok_s, tok_r, rs_s, rs_r, cell_s, cell_r, y_s, y_r, dn_s, dn_r,
 ):
@@ -173,8 +173,13 @@
         c.start()
 
     def up_rows(i):
-        off = i + (i // 2) * (5 - 2 * i) if n_kv == 4 else i
-        j = (kv + off) % n_kv
+        if n_kv == 4:
+            far_side = kv // 2
+            near = kv + far_side * (3 - 2 * kv)
+            step = (i + near) % 2 if i < 2 else i
+            j = 3 * far_side + (1 - 2 * far_side) * step
+        else:
+            j = (kv + i) % n_kv
         return j, pl.ds(pl.multiple_of(j * span, span), span)
 
     def up_copy(i):
@@ -213,17 +218,38 @@
             far_tok(o, t)[1].start()
 
     snd[:, heads : 2 * heads, :] = jnp.zeros((n_kv, heads, LANES), F32)
+    for c in small[1:]:
+        c.wait()
+
+    def chunk(t):
+        cols = pl.ds(pl.multiple_of((kv * n_tp + t) * thin, thin), thin)
+        raw = tokall[kv * n_tp + t].astype(F32)
+        return (raw * mixg[:, cols]).astype(BF16), jnp.sum(raw * raw, axis=1, keepdims=True)
+
+    def product(x, t, w):
+        rows = pl.ds(pl.multiple_of(t * thin, thin), thin)
+        return jnp.dot(x, w[rows, :], preferred_element_type=F32)
+
+    x_own, squares = chunk(tp)
+    for c in big[:3]:
+        c.wait()
+    for i in range(n_kv):
+        up_copy(i).start()
+    big[5].start()
+    own_parts = [product(x_own, tp, w) for w in (wq, wk, wv)]
     for src in mate:
         tok_wait(src)
-    for c in small[1:]:
-        c.wait()
-
-    def chunk(t):
-        return tokall[kv * n_tp + t].astype(F32)
-
-    raw = jnp.concatenate([chunk(t) for t in range(n_tp)], axis=1)
-    x = (raw * mixg[:, own_span]).astype(BF16)
-    squares = jnp.sum(raw * raw, axis=1, keepdims=True)
+    others = [((tp + t) % n_tp, chunk((tp + t) % n_tp)) for t in range(1, n_tp)]
+    for _, (_, more) in others:
+        squares = squares + more
+
+    def finished(n, w):
+        total = own_parts[n]
+        for t, (x_t, _) in others:
+            total = total + product(x_t, t, w)
+        return total
+
+    x = jnp.concatenate([chunk(t)[0] for t in range(n_tp)], axis=1)
     snd[:, heads + 2, :] = jnp.broadcast_to(squares, (n_kv, LANES))
     gate_count = wig.shape[0]
     last = (((1,), (1,)), ((), ()))
@@ -242,31 +268,23 @@
             device_id=(dp, to, tp), device_id_type=MESH)
 
     far_first = sorted(range(1, n_kv), key=lambda o: -min(o, n_kv - o))
-    big[0].wait()
-    q_part = jnp.dot(x, wq[...], preferred_element_type=F32)
+    q_part = finished(0, wq)
     for h in range(heads):
         snd[:, h, :] = q_part[:, h * dqk : (h + 1) * dqk]
     for o in far_first:
         rs_copy(o, 0).start()
-    big[1].wait()
-    up_copy(0).start()
-    up_copy(1).start()
-    k_part = jnp.dot(x, wk[...], preferred_element_type=F32)
+    k_part = finished(1, wk)
     for h in range(heads):
         snd[:, 2 * heads + h, :] = k_part[:, h * dqk : (h + 1) * dqk]
     for o in far_first:
         rs_copy(o, 1).start()
-    big[2].wait()
-    for i in range(2, n_kv):
-        up_copy(i).start()
-    v_part = jnp.dot(x, wv[...], preferred_element_type=F32)
+    v_part = finished(2, wv)
     for h in range(heads):
         for s in range(halves):
             at = h * dv + s * LANES
             snd[:, (3 + s) * heads + h, :] = v_part[:, at : at + LANES]
     for o in far_first:
         rs_copy(o, 2).start()
-    big[5].start()
     big[3].wait()
     membf[...] = mem[...].astype(BF16).reshape(heads * dv, dqk)
 
@@ -319,6 +337,7 @@
     v_rows = joined(2)
     v = jnp.concatenate([v_rows[s * heads : (s + 1) * heads] * scale for s in range(halves)], axis=1)
     cell = (keep * recall + (fresh * match) * v) / floor_value
+    cell = cell.astype(BF16)
     cell_own[...] = cell
 
     def cell_copy(o):
@@ -341,7 +360,8 @@
         pltpu.make_async_remote_copy(
             src_ref=cell_own, dst_ref=cell_all.at[src], send_sem=cell_s.at[o], recv_sem=cell_r.at[o],
             device_id=(dp, src, tp), device_id_type=MESH).wait_recv()
-    rows = jnp.concatenate([cell_all[:, h, :] for h in range(heads)], axis=1).astype(BF16)
+    cells = cell_all[...].astype(F32)
+    rows = jnp.concatenate([cells[:, h, :] for h in range(heads)], axis=1).astype(BF16)
     y = jnp.dot(rows, wo[...], preferred_element_type=F32).astype(BF16)
     y_own[...] = y
 
@@ -366,14 +386,13 @@
             src_ref=y_own, dst_ref=y_all.at[src], send_sem=y_s.at[0], recv_sem=y_r.at[src],
             device_id=peer_of(1)[1], device_id_type=MESH).wait_recv()
 
-    def up_step(i, square_sum):
+    def up_step(i, square_sum, total_up):
         j, span_rows = up_rows(i)
         up_copy(i).wait()
         for t in range(1, n_tp):
             y_wait(j * n_tp + (tp + t) % n_tp)
 
-        @pl.when(i > 0)
-        def _():
+        if i > 0:
             y_wait(j * n_tp + tp)
 
         base = jnp.concatenate([tokall[j * n_tp + t].astype(F32) for t in range(n_tp)], axis=1)
@@ -384,45 +403,37 @@
         mixed = (m * mlpg[:, span_rows]).astype(BF16)
         part = jnp.dot(mixed, wup[span_rows, :], preferred_element_type=F32)
 
-        @pl.when(i == 0)
-        def _():
-            acc[...] = part
-
-        @pl.when(i > 0)
-        def _():
-            acc[...] += part
-
-        return square_sum + jnp.sum(m * m, axis=1, keepdims=True)
-
-    square_sum = lax.fori_loop(0, n_kv, up_step, jnp.zeros((batch, 1), F32))
+        total_up = part if total_up is None else total_up + part
+        return square_sum + jnp.sum(m * m, axis=1, keepdims=True), total_up
+
+    square_sum = jnp.zeros((batch, 1), F32)
+    total_up = None
+    for i in range(n_kv):
+        square_sum, total_up = up_step(i, square_sum, total_up)
     scale2 = lax.rsqrt(square_sum * (1.0 / width) + norm_eps)
-    up = jnp.maximum(acc[...] * scale2, 0.0)
+    up = jnp.maximum(total_up * scale2, 0.0)
     act[...] = (up * up).astype(BF16)
     big[5].wait()
 
-    def dn_copy(o):
+    def dn_copy(to, src):
         return pltpu.make_async_remote_copy(
-            src_ref=stage.at[o], dst_ref=land.at[o], send_sem=dn_s.at[o], recv_sem=dn_r.at[o],
-            device_id=peer_of(o)[1], device_id_type=MESH)
-
-    def down_step(i, carry):
-        o = 1 + (i + n_all // 2 - 1) % (n_all - 1) + (i // (n_all - 1)) * (n_all - 1 - (n_all // 2 - 1))
-        o = o % n_all
-        other, _ = peer_of(o)
-        cols = pl.ds(pl.multiple_of(other * thin, thin), thin)
-        stage[o] = jnp.dot(act[...], wdn[:, cols], preferred_element_type=F32)
-
-        @pl.when(i < n_all - 1)
-        def _():
-            dn_copy(o).start()
-
-        return carry
-
-    lax.fori_loop(0, n_all, down_step, 0)
-    total = mid[kv, :, pl.ds(pl.multiple_of(tp * thin, thin), thin)] + stage[0]
-    for o in range(1, n_all):
-        dn_copy(o).wait_recv()
-        total = total + land[o]
+            src_ref=stage.at[to], dst_ref=land.at[src], send_sem=dn_s.at[to], recv_sem=dn_r.at[src],
+            device_id=(dp, to // n_tp, to % n_tp), device_id_type=MESH)
+
+    targets = [
+        up_rows(i)[0] * n_tp + (tp + t) % n_tp
+        for i in reversed(range(n_kv)) for t in reversed(range(n_tp))
+    ]
+    for to in targets[:-1]:
+        cols = pl.ds(pl.multiple_of(to * thin, thin), thin)
+        stage[to] = jnp.dot(act[...], wdn[:, cols], preferred_element_type=F32)
+        dn_copy(to, g).start()
+    own_cols = pl.ds(pl.multiple_of(g * thin, thin), thin)
+    total = jnp.dot(act[...], wdn[:, own_cols], preferred_element_type=F32)
+    total = total + mid[kv, :, pl.ds(pl.multiple_of(tp * thin, thin), thin)]
+    for src in reversed(targets[:-1]):
+        dn_copy(src, src).wait_recv()
+        total = total + land[src]
     otok[...] = total.astype(BF16)
 
     for src in mate:
@@ -439,8 +450,8 @@
             for p in range(len(pieces)):
                 rs_copy(o, p).wait_send()
             cell_copy(o).wait_send()
-    for o in range(1, n_all):
-        dn_copy(o).wait_send()
+    for to in targets[:-1]:
+        dn_copy(to, g).wait_send()
 
 
 def hand_over(a, b, c, d, out_a, out_b, out_c, out_d, sems):
@@ -504,12 +515,11 @@
         vm(w_down.shape, BF16),
         vm((n_kv, groups, LANES), F32),
         vm((n_kv, groups, LANES), F32),
-        vm((heads, dv), F32),
-        vm((n_kv, heads, dv), F32),
+        vm((heads, dv), BF16),
+        vm((n_kv, heads, dv), BF16),
         vm((batch, span), BF16),
         vm((n_all, batch, span), BF16),
         vm((n_kv, batch, span), F32),
-        vm((batch, hidden), F32),
         vm((batch, hidden), BF16),
         vm((n_all, batch, thin), F32),
         vm((n_all, batch, thin), F32),

time: 30.4 us -> 28.7 us (0.944)
  Pallas kernels: 29.6 us -> 27.9 us
    pallas_call x1, Pallas kernels: 28.6 us -> 26.9 us  [fused_on_device(): pl.pallas_call(functools.partial(fused_cell, n_kv, n_tp), out_shape=(jax....]
where the time goes in v3:
time: 28.7 us; the launch traced here: 28.6 us
  Pallas kernels  27.9 us (97%)
  between operations  0.65 us (2%)
    pallas_call x1, Pallas kernels, fused_on_device(): pl.pallas_call(functools.partial(fused_cell, n_kv, n_tp), out_shape=(jax....  26.9 us
    pallas_call x1, Pallas kernels, fused_on_device(): pl.pallas_call(hand_over, out_shape=tuple((jax.ShapeDtypeStruct(r.shape,...  1.01 us

profile of v3, /device:TPU:0, one launch (start us, length us, event | category | flops | bytes accessed | tf_op | source)
XLA Modules:
  0.0 28.6 jit_solution(17155396232808944564)
XLA Ops:
  0.6 26.9 %fused_cell.1 = (bf16[4,512]{1,0:T(4,128)(2,1)S(1)}, f32[1,8,256,128]{3,2,1,0:T(8,128)S(1)}, f32[1,8,128]{2,1,0:T(8,128)S(1)}, f32[1,8]{1,0:T(1,128)S(1)}) custom-call(bf16[4,512]{1,0:T(4,128)(2,1)} %tok_h.1, f32[1,4096]{1,0:T(1,128)} %bitcast.8, bf16[1024,1024]{1,0:T(8,128)(2,1)} %wq_h.1, bf16[1024,1024]{1,0:T(8,128)(2,1)} %wk_h.1, ...), custom_call_target="tpu_custom_call" | custom-call | tf_op jit(solution)/shard_map/fused_cell/pallas_call | solution.py:539
  27.5 1.0 %hand_over.1 = (bf16[4,512]{1,0:T(4,128)(2,1)}, f32[1,8,256,128]{3,2,1,0:T(8,128)}, f32[1,8,128]{2,1,0:T(8,128)}, f32[1,8]{1,0:T(1,128)}) custom-call(bf16[4,512]{1,0:T(4,128)(2,1)S(1)} %get-tuple-element.8.a, f32[1,8,256,128]{3,2,1,0:T(8,128)S(1)} %get-tuple-element.9.b, f32[1,8,128]{2,1,0:T(8,128)S(1)} %get-tuple-element.10.c, f32[1,8]{1,0:T(1,128)S(1)} %get-tuple-element.11.d), custom_call_target="tpu_custom_call" | custom-call | tf_op jit(solution)/shard_map/hand_over/pallas_call | solution.py:555
